TPU v7x, 32 devices: a whole 2x2x4 slice. The times are simulated.
32 devices in a mesh: sp: 8 (over z, y), dp: 4 (over x, core).
Axes of the slice: x: 2, y: 2, z: 4, core: 2. Of those that a mesh axis runs over, the one named last changes fastest.
Arguments:
- tokens: bfloat16 [4, 2560, 2048], P('dp', 'sp'), may hold values from -6 to 6
- w_query: bfloat16 [2048, 1024], P('dp', 'sp'), may hold values from -0.125 to 0.125
- w_key: bfloat16 [2048, 1024], P('dp', 'sp'), may hold values from -0.125 to 0.125
- w_value: bfloat16 [2048, 1024], P('dp', 'sp'), may hold values from -0.125 to 0.125
- w_output: bfloat16 [1024, 2048], P('sp', 'dp'), may hold values from -0.1875 to 0.1875
- qk_gain: float32 [2, 64], replicated, may hold values from 0.4 to 7
- decay_sums: float32 [4, 16, 2560], P('dp', 'sp'), may hold values from -512 to 0, as said below
Outputs:
- layer_out: bfloat16 [4, 2560, 2048], P('dp', 'sp')
Inputs may be any that keep to these rules, and one draw needn't show every extreme that they name: `decay_sums`: each row is non-increasing along positions.
All inputs are finite; a program needn't handle non-finite values.
Results may differ from a plain program's by a relative error of at most 0.0075.
The roundings to bfloat16 on the way count: a program that leaves them out, or rounds other values in their place, can miss the bound.
Values may be sent and summed in bfloat16 or wider, within the bound.
A program may use at most 128 MiB of HBM per device.

v0:
```python
import jax
import jax.numpy as jnp
from jax import lax
from jax.sharding import PartitionSpec as P


def normalize(values):
    values = values.astype(jnp.float32)
    return values * lax.rsqrt(jnp.mean(values * values, axis=-1, keepdims=True) + 1e-06)


def attend(query_unit, key_unit, value_rows, decay_rows):
    length = query_unit.shape[0]
    groups = query_unit.shape[1]
    width = query_unit.shape[2]
    block = min(512, length)

    def one_block(index):
        start = index * block
        query_block = lax.dynamic_slice_in_dim(query_unit, start, block, 0)
        decay_block = lax.dynamic_slice_in_dim(decay_rows, start, block, 1)
        query_place = start + jnp.arange(block, dtype=jnp.int32)

        def fill(column, buffer):
            key_start = column * block
            key_block = lax.dynamic_slice_in_dim(key_unit, key_start, block, 0)
            decay_keys = lax.dynamic_slice_in_dim(decay_rows, key_start, block, 1)
            scores = jnp.einsum(
                "qhd,khd->hqk", query_block, key_block, preferred_element_type=jnp.float32
            )
            scores = scores + decay_block[:, :, None] - decay_keys[:, None, :]
            key_place = key_start + jnp.arange(block, dtype=jnp.int32)
            scores = jnp.where(
                key_place[None, None, :] <= query_place[None, :, None], scores, -jnp.inf
            )
            return lax.dynamic_update_slice_in_dim(buffer, scores, key_start, 2)

        empty = jnp.full((groups, block, length), -jnp.inf, jnp.float32)
        scores = lax.fori_loop(0, index + 1, fill, empty)
        peak = jnp.max(scores, axis=-1, keepdims=True)
        weights = jnp.exp(scores - peak)
        probs = (weights / jnp.sum(weights, axis=-1, keepdims=True)).astype(jnp.bfloat16)

        def gather_values(column, running):
            key_start = column * block
            prob_block = lax.dynamic_slice_in_dim(probs, key_start, block, 2)
            value_block = lax.dynamic_slice_in_dim(value_rows, key_start, block, 0)
            return running + jnp.einsum(
                "hqk,khd->qhd", prob_block, value_block, preferred_element_type=jnp.float32
            )

        zeros = jnp.zeros((block, groups, width), jnp.float32)
        return lax.fori_loop(0, index + 1, gather_values, zeros)

    blocks = lax.map(one_block, jnp.arange(length // block, dtype=jnp.int32))
    return blocks.reshape(length, groups, width)


def on_device(tokens, w_query, w_key, w_value, w_output, qk_gain, decay_sums):
    own_rows = tokens[0]
    decay_rows = decay_sums[0]
    head_group = decay_rows.shape[0]
    head_dim = qk_gain.shape[1]
    stacked = jnp.stack((w_query, w_key, w_value))
    columns, out_columns = (
        lax.all_gather(stacked, "dp", axis=1, tiled=True),
        lax.all_gather(w_output, "dp", axis=1, tiled=True),
    )
    whole = lax.all_gather(own_rows, "sp", axis=0, tiled=True)
    triple = jnp.einsum("td,kdc->ktc", whole, columns, preferred_element_type=jnp.float32).astype(
        jnp.bfloat16
    )
    length = triple.shape[1]
    grouped = triple.reshape(3, length, head_group, head_dim)
    query_unit = (normalize(grouped[0]) * qk_gain[0] * head_dim ** (-0.5)).astype(jnp.bfloat16)
    key_unit = (normalize(grouped[1]) * qk_gain[1]).astype(jnp.bfloat16)
    attended = attend(query_unit, key_unit, grouped[2], decay_rows)
    head_out = normalize(attended).astype(jnp.bfloat16).reshape(length, head_group * head_dim)
    merged = lax.all_to_all(head_out, "sp", split_axis=0, concat_axis=1, tiled=True)
    result = jnp.dot(
        merged,
        lax.all_gather(out_columns, "sp", axis=0, tiled=True),
        preferred_element_type=jnp.float32,
    )
    return result.astype(jnp.bfloat16)[None]


def solution(mesh):
    placed = (
        P("dp", "sp", None),
        P("dp", "sp"),
        P("dp", "sp"),
        P("dp", "sp"),
        P("sp", "dp"),
        P(),
        P("dp", "sp", None),
    )
    return jax.shard_map(
        on_device, mesh=mesh, in_specs=placed, out_specs=P("dp", "sp", None), check_vma=False
    )
```

profile of v0, /device:TPU:29, one launch (start us, length us, event | category | flops | bytes accessed | tf_op | source)
XLA Modules:
  0.0 409.2 jit_solution(10661305282785432766)
XLA Ops:
  11.3 8.1 %all_gather.14 = bf16[128,2048]{1,0:T(8,128)(2,1)} all-gather(bf16[128,512]{1,0:T(8,128)(2,1)S(1)} %copy-done.1), channel_id=1, replica_groups=mesh['sp'=8,'dp'=4] {'dp'}, dimensions={1}, use_global_device_ids=true | all-gather | bytes 655360 | tf_op jit(solution)/shard_map/all_gather | solution.py:67
  19.4 12.1 %all-gather.5.cloned.1.call-done = bf16[3,2048,128]{1,2,0:T(8,128)(2,1)} async-done(((bf16[3,512,128]{1,2,0:T(8,128)(2,1)}), bf16[3,2048,128]{1,2,0:T(8,128)(2,1)}) %all-gather.5.cloned.1.call-update) | async-done | bytes 1572880 | tf_op jit(solution)/shard_map/all_gather | solution.py:66
  31.6 149.6 %all-gather.9.cloned.1.call-done = bf16[1,2560,2048]{2,1,0:T(8,128)(2,1)} async-done(((bf16[1,320,2048]{2,1,0:T(8,128)(2,1)}), bf16[1,2560,2048]{2,1,0:T(8,128)(2,1)}) %all-gather.9.cloned.1.call-update) | async-done | bytes 10485776 | tf_op jit(solution)/shard_map/all_gather | solution.py:69
  181.1 8.7 %fusion.17 = bf16[3,2560,128]{1,2,0:T(8,128)(2,1)S(1)} fusion(bf16[3,2048,128]{1,2,0:T(8,128)(2,1)} %all-gather.5.cloned.1.call-done, bf16[1,2560,2048]{2,1,0:T(8,128)(2,1)} %all-gather.9.cloned.1.call-done), kind=kOutput, calls=%fused_computation.25 | convolution fusion | flops 4027514880 | bytes 14024704 | tf_op jit(solution)/shard_map/td,kdc->ktc/dot_general | solution.py:70
  190.8 176.2 %while.33 = (s32[]{:T(128)}, f32[5,512,2,64]{1,3,2,0:T(8,128)S(1)}, s32[5]{0:T(128)S(1)}, bf16[2560,2,64]{0,2,1:T(8,128)(2,1)S(1)}, f32[2,2560]{1,0:T(2,128)}, /...) while((s32[]{:T(128)}, f32[5,512,2,64]{1,3,2,0:T(8,128)S(1)}, ...), condition=%wide.region_9.10_spmd, body=%wide.region_2.9_spmd.sunk | while | flops 143990816 | bytes 31886096 | solution.py:55
  193.5 5.3 %broadcast.99 = f32[2,512,2560]{1,2,0:T(8,128)} broadcast(f32[]{:T(128)} %constant.14.clone.6..sunk), dimensions={} | broadcast | bytes 10485764 | tf_op jit(solution)/shard_map/broadcast.5
  198.9 2.9 while.34
  199.8 2.0 fusion.46
  201.8 13.8 %divide_convert_fusion.2 = bf16[2,512,2560]{1,2,0:T(8,128)(2,1)} fusion(f32[2,512,2560]{1,2,0:T(8,128)} %get-tuple-element.345), kind=kOutput, calls=%fused_computation.16.clone.1 | output fusion | flops 7871486 | bytes 15728640 | tf_op jit(solution)/shard_map/while/body/eval_jaxpr/div | solution.py:42
  219.8 5.3 %broadcast.99 = f32[2,512,2560]{1,2,0:T(8,128)} broadcast(f32[]{:T(128)} %constant.14.clone.6..sunk), dimensions={} | broadcast | bytes 10485764 | tf_op jit(solution)/shard_map/broadcast.5
  225.1 5.8 %while.34 = (s32[]{:T(128)}, f32[2,512,2560]{1,2,0:T(8,128)}, s32[]{:T(128)}, bf16[2560,2,64]{0,2,1:T(8,128)(2,1)S(1)}, bf16[512,2,64]{0,2,1:T(8,128)(2,1)S(1)},...) while((s32[]{:T(128)}, f32[2,512,2560]{1,2,0:T(8,128)}, ...), condition=%wide.region_4.4_spmd.clone, body=%wide.region_3.3_spmd.clone.sunk | while | flops 68944904 | bytes 2909359 | solution.py:39
  230.9 13.8 %divide_convert_fusion.2 = bf16[2,512,2560]{1,2,0:T(8,128)(2,1)} fusion(f32[2,512,2560]{1,2,0:T(8,128)} %get-tuple-element.345), kind=kOutput, calls=%fused_computation.16.clone.1 | output fusion | flops 7871486 | bytes 15728640 | tf_op jit(solution)/shard_map/while/body/eval_jaxpr/div | solution.py:42
  244.8 3.1 while.35
  250.5 5.3 %broadcast.99 = f32[2,512,2560]{1,2,0:T(8,128)} broadcast(f32[]{:T(128)} %constant.14.clone.6..sunk), dimensions={} | broadcast | bytes 10485764 | tf_op jit(solution)/shard_map/broadcast.5
  255.8 8.7 %while.34 = (s32[]{:T(128)}, f32[2,512,2560]{1,2,0:T(8,128)}, s32[]{:T(128)}, bf16[2560,2,64]{0,2,1:T(8,128)(2,1)S(1)}, bf16[512,2,64]{0,2,1:T(8,128)(2,1)S(1)},...) while((s32[]{:T(128)}, f32[2,512,2560]{1,2,0:T(8,128)}, ...), condition=%wide.region_4.4_spmd.clone, body=%wide.region_3.3_spmd.clone.sunk | while | flops 68944904 | bytes 2909359 | solution.py:39
  256.8 2.0 fusion.46
  264.5 13.8 %divide_convert_fusion.2 = bf16[2,512,2560]{1,2,0:T(8,128)(2,1)} fusion(f32[2,512,2560]{1,2,0:T(8,128)} %get-tuple-element.345), kind=kOutput, calls=%fused_computation.16.clone.1 | output fusion | flops 7871486 | bytes 15728640 | tf_op jit(solution)/shard_map/while/body/eval_jaxpr/div | solution.py:42
  278.4 4.7 %while.35 = (s32[]{:T(128)}, f32[512,2,64]{0,2,1:T(8,128)S(1)}, s32[]{:T(128)}, bf16[2560,2,64]{0,2,1:T(8,128)(2,1)S(1)}, bf16[2,512,2560]{1,2,0:T(8,128)(2,1)},...) while((s32[]{:T(128)}, f32[512,2,64]{0,2,1:T(8,128)S(1)}, s32[]{:T(128)}, ...), condition=%wide.region_8.8_spmd, body=%wide.region_7.7_spmd.sunk | while | flops 67174408 | bytes 1705099 | solution.py:53
  285.7 5.3 %broadcast.99 = f32[2,512,2560]{1,2,0:T(8,128)} broadcast(f32[]{:T(128)} %constant.14.clone.6..sunk), dimensions={} | broadcast | bytes 10485764 | tf_op jit(solution)/shard_map/broadcast.5
  291.0 11.7 %while.34 = (s32[]{:T(128)}, f32[2,512,2560]{1,2,0:T(8,128)}, s32[]{:T(128)}, bf16[2560,2,64]{0,2,1:T(8,128)(2,1)S(1)}, bf16[512,2,64]{0,2,1:T(8,128)(2,1)S(1)},...) while((s32[]{:T(128)}, f32[2,512,2560]{1,2,0:T(8,128)}, ...), condition=%wide.region_4.4_spmd.clone, body=%wide.region_3.3_spmd.clone.sunk | while | flops 68944904 | bytes 2909359 | solution.py:39
  300.6 2.1 fusion.46
  302.7 13.8 %divide_convert_fusion.2 = bf16[2,512,2560]{1,2,0:T(8,128)(2,1)} fusion(f32[2,512,2560]{1,2,0:T(8,128)} %get-tuple-element.345), kind=kOutput, calls=%fused_computation.16.clone.1 | output fusion | flops 7871486 | bytes 15728640 | tf_op jit(solution)/shard_map/while/body/eval_jaxpr/div | solution.py:42
  316.5 6.3 %while.35 = (s32[]{:T(128)}, f32[512,2,64]{0,2,1:T(8,128)S(1)}, s32[]{:T(128)}, bf16[2560,2,64]{0,2,1:T(8,128)(2,1)S(1)}, bf16[2,512,2560]{1,2,0:T(8,128)(2,1)},...) while((s32[]{:T(128)}, f32[512,2,64]{0,2,1:T(8,128)S(1)}, s32[]{:T(128)}, ...), condition=%wide.region_8.8_spmd, body=%wide.region_7.7_spmd.sunk | while | flops 67174408 | bytes 1705099 | solution.py:53
  325.4 5.3 %broadcast.99 = f32[2,512,2560]{1,2,0:T(8,128)} broadcast(f32[]{:T(128)} %constant.14.clone.6..sunk), dimensions={} | broadcast | bytes 10485764 | tf_op jit(solution)/shard_map/broadcast.5
  330.7 14.5 %while.34 = (s32[]{:T(128)}, f32[2,512,2560]{1,2,0:T(8,128)}, s32[]{:T(128)}, bf16[2560,2,64]{0,2,1:T(8,128)(2,1)S(1)}, bf16[512,2,64]{0,2,1:T(8,128)(2,1)S(1)},...) while((s32[]{:T(128)}, f32[2,512,2560]{1,2,0:T(8,128)}, ...), condition=%wide.region_4.4_spmd.clone, body=%wide.region_3.3_spmd.clone.sunk | while | flops 68944904 | bytes 2909359 | solution.py:39
  340.3 2.1 fusion.46
  345.3 13.8 %divide_convert_fusion.2 = bf16[2,512,2560]{1,2,0:T(8,128)(2,1)} fusion(f32[2,512,2560]{1,2,0:T(8,128)} %get-tuple-element.345), kind=kOutput, calls=%fused_computation.16.clone.1 | output fusion | flops 7871486 | bytes 15728640 | tf_op jit(solution)/shard_map/while/body/eval_jaxpr/div | solution.py:42
  359.1 7.9 %while.35 = (s32[]{:T(128)}, f32[512,2,64]{0,2,1:T(8,128)S(1)}, s32[]{:T(128)}, bf16[2560,2,64]{0,2,1:T(8,128)(2,1)S(1)}, bf16[2,512,2560]{1,2,0:T(8,128)(2,1)},...) while((s32[]{:T(128)}, f32[512,2,64]{0,2,1:T(8,128)S(1)}, s32[]{:T(128)}, ...), condition=%wide.region_8.8_spmd, body=%wide.region_7.7_spmd.sunk | while | flops 67174408 | bytes 1705099 | solution.py:53
  373.9 2.4 copy.29
  376.3 6.0 %all-to-all-start = ((bf16[8,320,128]{2,1,0:T(8,128)(2,1)}), bf16[8,320,128]{2,1,0:T(8,128)(2,1)S(1)}, u32[]{:S(2)}, u32[]{:S(2)}) async-start(bf16[8,320,128]{2,1,0:T(8,128)(2,1)} %copy.29), calls=%async_computation | async-start | bytes 1310720 | tf_op jit(solution)/shard_map/all_to_all | solution.py:79
  382.3 15.6 %all-to-all-done = bf16[8,320,128]{2,1,0:T(8,128)(2,1)S(1)} async-done(((bf16[8,320,128]{2,1,0:T(8,128)(2,1)}), bf16[8,320,128]{2,1,0:T(8,128)(2,1)S(1)}, u32[]{:S(2)}, u32[]{:S(2)}) %all-to-all-start) | async-done | bytes 655392 | tf_op jit(solution)/shard_map/all_to_all | solution.py:79
  397.9 4.8 %fusion.20 = bf16[1,320,2048]{2,1,0:T(8,128)(2,1)} fusion(bf16[1024,2048]{1,0:T(8,128)(2,1)} %all-gather.7.cloned.1.call-done, bf16[8,320,128]{2,1,0:T(8,128)(2,1)S(1)} %all-to-all-done), kind=kOutput, calls=%fused_computation.27 | convolution fusion | flops 1342832640 | bytes 6160384 | tf_op jit(solution)/shard_map/dot_general | solution.py:80
  (130 shorter events, 79.1 us)
Async XLA Ops:
  6.5 4.7 %copy-start.1 = (bf16[128,512]{1,0:T(8,128)(2,1)S(1)}, bf16[128,512]{1,0:T(8,128)(2,1)}, u32[]{:S(2)}) copy-start(bf16[128,512]{1,0:T(8,128)(2,1)} %param.17) | copy-start | bytes 393220
  6.5 25.0 %all-gather.5.cloned.1.call-start = ((), (), s32[]{:S(2)}) async-start(), calls=%async_computation.1 | async-start | bytes 1966080 | tf_op jit(solution)/shard_map/all_gather | solution.py:66
  8.6 10.8 %copy-start.2 = (f32[2,64]{1,0:T(2,128)S(1)}, f32[2,64]{1,0:T(2,128)}, u32[]{:S(2)}) copy-start(f32[2,64]{1,0:T(2,128)} %param.18) | copy-start | bytes 1540
  10.4 170.7 %all-gather.9.cloned.1.call-start = ((), (), s32[]{:S(2)}) async-start(), calls=%async_computation.3 | async-start | bytes 11796480 | tf_op jit(solution)/shard_map/all_gather | solution.py:69
  11.2 371.1 %all-gather.7.cloned.1.call-start = ((), (), s32[]{:S(2)}) async-start(), calls=%async_computation.2 | async-start | bytes 4718592 | tf_op jit(solution)/shard_map/all_gather | solution.py:82
  370.0 2.9 copy-start
  376.3 21.7 %all-to-all-start = ((bf16[8,320,128]{2,1,0:T(8,128)(2,1)}), bf16[8,320,128]{2,1,0:T(8,128)(2,1)S(1)}, u32[]{:S(2)}, u32[]{:S(2)}) async-start(bf16[8,320,128]{2,1,0:T(8,128)(2,1)} %copy.29), calls=%async_computation | async-start | bytes 1310720 | tf_op jit(solution)/shard_map/all_to_all | solution.py:79
Sparse Core Ops, SparseCore 0:
  10.6 20.9 all-gather.4
  33.7 147.3 all-gather.8
  183.3 71.3 all-gather.6
where the time goes:
time: 414 us; the launch traced here: 409 us
  waiting for transfers between devices  178 us (43%)
  other arithmetic  75.1 us (18%)
  matrix products  66.4 us (16%)
  local copies, waits for them, and re-layouts  54.8 us (13%)
  between operations  13.3 us (3%)
  blocking collectives  8.13 us (2%)
  loops' own time  7.36 us (2%)
  starting transfers between devices  6.1 us (1%)
    all_gather x1, waiting for transfers between devices, on_device(): whole = lax.all_gather(own_rows, 'sp', axis=0, tiled=True)  150 us
    div x5, other arithmetic, one_block(): weights / jnp.sum(weights, axis=-1, keepdims=True)  69 us
    dot_general x15, matrix products, fill(): jnp.einsum('qhd,khd->hqk', query_block, key_block, preferred_element_type...  29.8 us
    another operation x10, local copies, waits for them, and re-layouts  26.7 us
    dot_general x15, matrix products, gather_values(): jnp.einsum('hqk,khd->qhd', prob_block, value_block, preferred_element_typ...  23.1 us
    all_to_all x1, waiting for transfers between devices, on_device(): lax.all_to_all(head_out, 'sp', split_axis=0, concat_axis=1, tiled=True)  15.6 us
    all_gather x1, waiting for transfers between devices, on_device(): lax.all_gather(stacked, 'dp', axis=1, tiled=True)  12.1 us
    dynamic_slice x15, local copies, waits for them, and re-layouts, fill(): decay_keys = lax.dynamic_slice_in_dim(decay_rows, key_start, block, 1)  10.3 us
  transfers between devices with their start and end apart: 4, of which 3 were waited for; matrix products, arithmetic and copies ran while one was open for 46% of the time, Pallas kernels for 0%

commit v1 on v0

v1 whole, which is shorter than its diff:
```python
import functools

import jax
import jax.numpy as jnp
from jax import lax
from jax.experimental import pallas as pl
from jax.experimental.pallas import tpu as pltpu
from jax.sharding import PartitionSpec as P

EPS = 1e-06
DIMS_NT = (((1,), (1,)), ((), ()))


def attention_kernel(
    heads, width, block, rows_ref, weight_ref, gain_ref, decay_ref, out_ref, key_ref, value_ref
):
    index = pl.program_id(0)
    wide = heads * width
    projected = jnp.dot(
        rows_ref[...], weight_ref[...], preferred_element_type=jnp.float32
    ).astype(jnp.bfloat16)
    place = pl.ds(pl.multiple_of(index * block, block), block)

    def unit(values, gain):
        values = values.astype(jnp.float32)
        scale = lax.rsqrt(jnp.mean(values * values, axis=-1, keepdims=True) + EPS)
        return values * scale * gain

    values_turned = projected[:, 2 * wide :].astype(jnp.float32).T
    lane = lax.broadcasted_iota(jnp.int32, (block, width), 1)
    ones_lanes = jnp.where(lane < 3, 1.0, 0.0)
    sub = lax.broadcasted_iota(jnp.int32, (2 * width, block), 0)
    ones_rows = jnp.where(
        lax.broadcasted_iota(jnp.int32, (16, block), 0) == 0, 1.0, 0.0
    )
    queries = []
    for head in range(heads):
        low = head * width
        query = unit(projected[:, low : low + width], gain_ref[0:1, :]) * width ** (-0.5)
        key = unit(projected[:, wide + low : wide + low + width], gain_ref[1:2, :])
        decay = -decay_ref[head : head + 1, :]
        first = decay.astype(jnp.bfloat16).astype(jnp.float32)
        rest = decay - first
        second = rest.astype(jnp.bfloat16).astype(jnp.float32)
        third = rest - second
        parts = jnp.where(
            sub == 0, first, jnp.where(sub == 1, second, jnp.where(sub == 2, third, 0.0))
        ).T
        queries.append(jnp.concatenate([query, ones_lanes], axis=1).astype(jnp.bfloat16))
        key_ref[head, place, :] = jnp.concatenate([key, parts[:, :width]], axis=1).astype(
            jnp.bfloat16
        )
        value_ref[head, index] = jnp.concatenate(
            [values_turned[low : low + width], ones_rows], axis=0
        ).astype(jnp.bfloat16)

    def step(column, carry, masked):
        fresh = []
        for head in range(heads):
            peak, total = carry[head]
            keys = key_ref[head, pl.ds(pl.multiple_of(column * block, block), block), :]
            scores = lax.dot_general(
                keys, queries[head], DIMS_NT, preferred_element_type=jnp.float32
            )
            if masked:
                key_place = lax.broadcasted_iota(jnp.int32, scores.shape, 0)
                query_place = lax.broadcasted_iota(jnp.int32, scores.shape, 1)
                scores = jnp.where(key_place <= query_place, scores, -jnp.inf)
            higher = jnp.maximum(peak, jnp.max(scores, axis=0, keepdims=True))
            probs = jnp.exp(scores - higher).astype(jnp.bfloat16)
            total = total * jnp.exp(peak - higher) + jnp.dot(
                value_ref[head, column], probs, preferred_element_type=jnp.float32
            )
            fresh.append((higher, total))
        return tuple(fresh)

    start = tuple(
        (
            jnp.full((1, block), -1e30, jnp.float32),
            jnp.zeros((width + 16, block), jnp.float32),
        )
        for _ in range(heads)
    )
    carry = step(index, start, True)
    carry = lax.fori_loop(0, index, lambda column, c: step(column, c, False), carry)
    outs = []
    for head in range(heads):
        total = carry[head][1]
        mixed, norm = total[:width], total[width : width + 1]
        scale = lax.rsqrt(jnp.mean(mixed * mixed, axis=0, keepdims=True) + EPS * norm * norm)
        outs.append(mixed * scale)
    out_ref[...] = jnp.concatenate(outs, axis=0).T.astype(jnp.bfloat16)


def attend(whole, weights, qk_gain, decay_rows):
    length, depth = whole.shape
    heads = decay_rows.shape[0]
    width = qk_gain.shape[1]
    block = 512
    steps = length // block
    wide = heads * width
    return pl.pallas_call(
        functools.partial(attention_kernel, heads, width, block),
        grid=(steps,),
        out_shape=jax.ShapeDtypeStruct((length, wide), jnp.bfloat16),
        in_specs=[
            pl.BlockSpec((block, depth), lambda i: (i, 0)),
            pl.BlockSpec((depth, 3 * wide), lambda i: (0, 0)),
            pl.BlockSpec((2, width), lambda i: (0, 0)),
            pl.BlockSpec((heads, block), lambda i: (0, i)),
        ],
        out_specs=pl.BlockSpec((block, wide), lambda i: (i, 0)),
        scratch_shapes=[
            pltpu.VMEM((heads, length, 2 * width), jnp.bfloat16),
            pltpu.VMEM((heads, steps, width + 16, block), jnp.bfloat16),
        ],
        compiler_params=pltpu.CompilerParams(vmem_limit_bytes=56 * 1024 * 1024),
        cost_estimate=pl.CostEstimate(
            flops=2 * length * depth * 3 * wide + 2 * heads * length * length * 2 * width,
            bytes_accessed=2 * length * depth,
            transcendentals=heads * length * length // 2,
        ),
    )(whole, weights, qk_gain, decay_rows)


def on_device(tokens, w_query, w_key, w_value, w_output, qk_gain, decay_sums):
    own_rows = tokens[0]
    stacked = jnp.concatenate((w_query, w_key, w_value), axis=1)
    columns = lax.all_gather(stacked, "dp", axis=0, tiled=True)
    whole = lax.all_gather(own_rows, "sp", axis=0, tiled=True)
    out_rows = lax.all_gather(w_output, "sp", axis=0, tiled=True)
    out_weight = lax.all_gather(out_rows, "dp", axis=1, tiled=True)
    head_out = attend(whole, columns, qk_gain, decay_sums[0])
    merged = lax.all_to_all(head_out, "sp", split_axis=0, concat_axis=1, tiled=True)
    result = jnp.dot(merged, out_weight, preferred_element_type=jnp.float32)
    return result.astype(jnp.bfloat16)[None]


def solution(mesh):
    placed = (
        P("dp", "sp", None),
        P("dp", "sp"),
        P("dp", "sp"),
        P("dp", "sp"),
        P("sp", "dp"),
        P(),
        P("dp", "sp", None),
    )
    return jax.shard_map(
        on_device, mesh=mesh, in_specs=placed, out_specs=P("dp", "sp", None), check_vma=False
    )
```

time: 414 us -> 291 us (0.70)
  other arithmetic: 75.1 us -> 1.83 us
  matrix products: 66.4 us -> 4.77 us
  local copies, waits for them, and re-layouts: 54.8 us -> 0 us
  waiting for transfers between devices: 178 us -> 228 us
  Pallas kernels: 0 us -> 33.9 us
  blocking collectives: 8.13 us -> 0 us
  loops' own time: 7.36 us -> 0 us
    div x5 -> x0, other arithmetic: 69 us -> none  [one_block(): weights / jnp.sum(weights, axis=-1, keepdims=True)]
    dot_general x32 -> x1, matrix products: 66.4 us -> 4.77 us  [on_device(): result = jnp.dot(merged, out_weight, preferred_element_type=jnp.float32)]
    all_gather x2 -> x3, waiting for transfers between devices: 12.1 us -> 61.1 us  [the longest x1 36.7 us: on_device(): out_rows = lax.all_gather(w_output, 'sp', axis=0, tiled=True)]
    pallas_call x0 -> x1, Pallas kernels: none -> 33.9 us  [attend(): pl.pallas_call(functools.partial(attention_kernel, heads, width, block),...]
    another operation x10 -> x0, local copies, waits for them, and re-layouts: 26.7 us -> none
    dynamic_slice x30 -> x0, local copies, waits for them, and re-layouts: 16.8 us -> none  [the longest x15 10.3 us: fill(): decay_keys = lax.dynamic_slice_in_dim(decay_rows, key_start, block, 1)]
    all_gather x1 -> x0, blocking collectives: 8.13 us -> none  [on_device(): lax.all_gather(w_output, 'dp', axis=1, tiled=True)]
    another operation x11 -> x0, loops' own time: 7.36 us -> none  [the longest x1 6.72 us: attend(): blocks = lax.map(one_block, jnp.arange(length // block, dtype=jnp.int32))]
  transfers between devices with their start and end apart: 4 -> 5, of which waited for: 3 -> 4; matrix products, arithmetic and copies ran while one was open for 46% -> 1% of each run, Pallas kernels for 0% -> 12%
where the time goes in v1:
time: 291 us; the launch traced here: 287 us
  waiting for transfers between devices  228 us (78%)
  Pallas kernels  33.9 us (12%)
  between operations  13.1 us (5%)
  starting transfers between devices  5.86 us (2%)
  matrix products  4.77 us (2%)
    all_gather x1, waiting for transfers between devices, on_device(): whole = lax.all_gather(own_rows, 'sp', axis=0, tiled=True)  150 us
    all_gather x1, waiting for transfers between devices, on_device(): out_rows = lax.all_gather(w_output, 'sp', axis=0, tiled=True)  36.7 us
    pallas_call x1, Pallas kernels, attend(): pl.pallas_call(functools.partial(attention_kernel, heads, width, block),...  33.9 us
    all_gather x1, waiting for transfers between devices, on_device(): columns = lax.all_gather(stacked, 'dp', axis=0, tiled=True)  24.4 us
    all_to_all x1, waiting for transfers between devices, on_device(): lax.all_to_all(head_out, 'sp', split_axis=0, concat_axis=1, tiled=True)  15.6 us
  transfers between devices with their start and end apart: 5, of which 4 were waited for; matrix products, arithmetic and copies ran while one was open for 1% of the time, Pallas kernels for 12%

profile of v1, /device:TPU:29, one launch (start us, length us, event | category | flops | bytes accessed | tf_op | source)
XLA Modules:
  0.0 287.2 jit_solution(5158663122069341790)
XLA Ops:
  6.5 0.0 all-gather.8.cloned.1.call-start
  6.5 0.7 all-gather.8.cloned.1.call-update
  7.3 0.0 all-gather.6.cloned.1.call-start
  7.3 1.8 pad_maximum_fusion
  9.1 0.0 all-gather.6.cloned.1.call-update
  9.2 0.0 all-gather.12.cloned.1.call-start
  9.2 0.7 all-gather.12.cloned.1.call-update
  9.9 0.0 all-gather.10.cloned.1.call-start
  9.9 36.7 %all-gather.8.cloned.1.call-done = bf16[1024,512]{1,0:T(8,128)(2,1)} async-done(((bf16[128,512]{1,0:T(8,128)(2,1)}), bf16[1024,512]{1,0:T(8,128)(2,1)}) %all-gather.8.cloned.1.call-update) | async-done | bytes 1048592 | tf_op jit(solution)/shard_map/all_gather | solution.py:131
  46.6 0.0 all-gather.10.cloned.1.call-update
  46.6 24.4 %all-gather.6.cloned.1.call-done.weight_ref = bf16[2048,384]{1,0:T(8,128)(2,1)} async-done(((bf16[512,384]{1,0:T(8,128)(2,1)}), bf16[2048,384]{1,0:T(8,128)(2,1)}) %all-gather.6.cloned.1.call-update) | async-done | bytes 1572880 | tf_op jit(solution)/shard_map/all_gather | solution.py:129
  71.0 149.6 %all-gather.12.cloned.1.call-done = bf16[1,2560,2048]{2,1,0:T(8,128)(2,1)} async-done(((bf16[1,320,2048]{2,1,0:T(8,128)(2,1)}), bf16[1,2560,2048]{2,1,0:T(8,128)(2,1)}) %all-gather.12.cloned.1.call-update) | async-done | bytes 10485776 | tf_op jit(solution)/shard_map/all_gather | solution.py:130
  220.6 33.9 %shard_map.73 = bf16[2560,128]{1,0:T(8,128)(2,1)} custom-call(bf16[2560,2048]{1,0:T(8,128)(2,1)} %bitcast.15, bf16[2048,384]{1,0:T(8,128)(2,1)} %all-gather.6.cloned.1.call-done.weight_ref, f32[2,64]{1,0:T(2,128)} %gain_ref.1, f32[2,2560]{1,0:T(2,128)} %bitcast.16), custom_call_target="tpu_custom_call" | custom-call | flops 7381975040 | bytes 10485760 | tf_op jit(solution)/shard_map/pallas_call | solution.py:102
  254.5 5.7 %all-to-all-start = ((bf16[8,320,128]{2,1,0:T(8,128)(2,1)}), bf16[8,320,128]{2,1,0:T(8,128)(2,1)S(1)}, u32[]{:S(2)}, u32[]{:S(2)}) async-start(bf16[8,320,128]{2,1,0:T(8,128)(2,1)} %bitcast.14), calls=%async_computation | async-start | bytes 1310720 | tf_op jit(solution)/shard_map/all_to_all | solution.py:134
  260.3 0.0 all-gather.10.cloned.1.call-done
  260.3 15.6 %all-to-all-done = bf16[8,320,128]{2,1,0:T(8,128)(2,1)S(1)} async-done(((bf16[8,320,128]{2,1,0:T(8,128)(2,1)}), bf16[8,320,128]{2,1,0:T(8,128)(2,1)S(1)}, u32[]{:S(2)}, u32[]{:S(2)}) %all-to-all-start) | async-done | bytes 655392 | tf_op jit(solution)/shard_map/all_to_all | solution.py:134
  275.9 4.8 %fusion = bf16[1,320,2048]{2,1,0:T(8,128)(2,1)} fusion(bf16[1024,2048]{1,0:T(8,128)(2,1)} %all-gather.10.cloned.1.call-done, bf16[8,320,128]{2,1,0:T(8,128)(2,1)S(1)} %all-to-all-done), kind=kOutput, calls=%fused_computation.1 | convolution fusion | flops 1342832640 | bytes 6160384 | tf_op jit(solution)/shard_map/dot_general | solution.py:135
Async XLA Ops:
  6.5 40.1 %all-gather.8.cloned.1.call-start = ((), (), s32[]{:S(2)}) async-start(), calls=%async_computation.2 | async-start | bytes 1179648 | tf_op jit(solution)/shard_map/all_gather | solution.py:131
  7.3 63.8 %all-gather.6.cloned.1.call-start = ((), (), s32[]{:S(2)}) async-start(), calls=%async_computation.1 | async-start | bytes 1966080 | tf_op jit(solution)/shard_map/all_gather | solution.py:129
  9.2 211.4 %all-gather.12.cloned.1.call-start = ((), (), s32[]{:S(2)}) async-start(), calls=%async_computation.4 | async-start | bytes 11796480 | tf_op jit(solution)/shard_map/all_gather | solution.py:130
  9.9 250.4 %all-gather.10.cloned.1.call-start = ((), (), s32[]{:S(2)}) async-start(), calls=%async_computation.3 | async-start | bytes 5242880 | tf_op jit(solution)/shard_map/all_gather | solution.py:132
  254.5 21.4 %all-to-all-start = ((bf16[8,320,128]{2,1,0:T(8,128)(2,1)}), bf16[8,320,128]{2,1,0:T(8,128)(2,1)S(1)}, u32[]{:S(2)}, u32[]{:S(2)}) async-start(bf16[8,320,128]{2,1,0:T(8,128)(2,1)} %bitcast.14), calls=%async_computation | async-start | bytes 1310720 | tf_op jit(solution)/shard_map/all_to_all | solution.py:134
Sparse Core Ops, SparseCore 0:
  9.5 37.1 all-gather.7
  48.2 22.7 all-gather.5
  73.2 147.3 all-gather.11
  222.0 35.7 all-gather.9

commit v2 on v1

--- a/solution.py
+++ b/solution.py
@@ -16,10 +16,10 @@
 ):
     index = pl.program_id(0)
     wide = heads * width
+    place = pl.ds(pl.multiple_of(index * block, block), block)
     projected = jnp.dot(
-        rows_ref[...], weight_ref[...], preferred_element_type=jnp.float32
+        rows_ref[place, :], weight_ref[...], preferred_element_type=jnp.float32
     ).astype(jnp.bfloat16)
-    place = pl.ds(pl.multiple_of(index * block, block), block)
 
     def unit(values, gain):
         values = values.astype(jnp.float32)
@@ -104,7 +104,7 @@
         grid=(steps,),
         out_shape=jax.ShapeDtypeStruct((length, wide), jnp.bfloat16),
         in_specs=[
-            pl.BlockSpec((block, depth), lambda i: (i, 0)),
+            pl.BlockSpec(memory_space=pltpu.VMEM),
             pl.BlockSpec((depth, 3 * wide), lambda i: (0, 0)),
             pl.BlockSpec((2, width), lambda i: (0, 0)),
             pl.BlockSpec((heads, block), lambda i: (0, i)),
@@ -114,7 +114,7 @@
             pltpu.VMEM((heads, length, 2 * width), jnp.bfloat16),
             pltpu.VMEM((heads, steps, width + 16, block), jnp.bfloat16),
         ],
-        compiler_params=pltpu.CompilerParams(vmem_limit_bytes=56 * 1024 * 1024),
+        compiler_params=pltpu.CompilerParams(vmem_limit_bytes=44 * 1024 * 1024),
         cost_estimate=pl.CostEstimate(
             flops=2 * length * depth * 3 * wide + 2 * heads * length * length * 2 * width,
             bytes_accessed=2 * length * depth,
@@ -123,12 +123,95 @@
     )(whole, weights, qk_gain, decay_rows)
 
 
+PIECES = 2
+
+
+def ring_kernel(count, own_ref, whole_ref, send_sem, recv_sem, local_sem):
+    rows = own_ref.shape[0]
+    part = rows // (2 * PIECES)
+    tall = 4 if count % 4 == 0 else 1
+    broad = count // tall
+
+    def member(spot):
+        spot = lax.rem(spot + 2 * count, count)
+        column, height = spot // tall, lax.rem(spot, tall)
+        level = height + lax.rem(column, 2) * (tall - 1 - 2 * height)
+        return level * broad + column
+
+    me = lax.axis_index("sp")
+    level, column = me // broad, lax.rem(me, broad)
+    spot = column * tall + level + lax.rem(column, 2) * (tall - 1 - 2 * level)
+    ways = (1, -1)
+    targets = [member(spot + way) for way in ways]
+
+    barrier = pltpu.get_barrier_semaphore()
+    for target in targets:
+        pl.semaphore_signal(
+            barrier, inc=1, device_id={"sp": target}, device_id_type=pl.DeviceIdType.MESH
+        )
+    pl.semaphore_wait(barrier, 2)
+
+    local = pltpu.make_async_copy(
+        own_ref, whole_ref.at[pl.ds(pl.multiple_of(me * rows, rows), rows)], local_sem
+    )
+    local.start()
+    copies = {}
+    for step in range(count - 1):
+        for piece in range(PIECES):
+            for side, way in enumerate(ways):
+                offset = (side * PIECES + piece) * part
+                if step:
+                    copies[step - 1, piece, side].wait_recv()
+                origin = member(spot - way * step)
+                place = pl.ds(pl.multiple_of(origin * rows + offset, part), part)
+                source = own_ref.at[pl.ds(offset, part)] if step == 0 else whole_ref.at[place]
+                copy = pltpu.make_async_remote_copy(
+                    src_ref=source,
+                    dst_ref=whole_ref.at[place],
+                    send_sem=send_sem.at[step, piece, side],
+                    recv_sem=recv_sem.at[step, piece, side],
+                    device_id={"sp": targets[side]},
+                    device_id_type=pl.DeviceIdType.MESH,
+                )
+                copy.start()
+                copies[step, piece, side] = copy
+    for piece in range(PIECES):
+        for side in range(2):
+            copies[count - 2, piece, side].wait_recv()
+    for copy in copies.values():
+        copy.wait_send()
+    local.wait()
+
+
+def gather_rows(own_rows, count):
+    rows, depth = own_rows.shape
+    shape = (count - 1, PIECES, 2)
+    return pl.pallas_call(
+        functools.partial(ring_kernel, count),
+        out_shape=jax.ShapeDtypeStruct((count * rows, depth), own_rows.dtype),
+        in_specs=[pl.BlockSpec(memory_space=pltpu.VMEM)],
+        out_specs=pl.BlockSpec(memory_space=pl.ANY),
+        scratch_shapes=[
+            pltpu.SemaphoreType.DMA(shape),
+            pltpu.SemaphoreType.DMA(shape),
+            pltpu.SemaphoreType.DMA,
+        ],
+        compiler_params=pltpu.CompilerParams(
+            collective_id=0, has_side_effects=True, vmem_limit_bytes=16 * 1024 * 1024
+        ),
+        cost_estimate=pl.CostEstimate(
+            flops=10**11, bytes_accessed=2 * count * rows * depth, transcendentals=0
+        ),
+    )(own_rows)
+
+
 def on_device(tokens, w_query, w_key, w_value, w_output, qk_gain, decay_sums):
     own_rows = tokens[0]
     stacked = jnp.concatenate((w_query, w_key, w_value), axis=1)
     columns = lax.all_gather(stacked, "dp", axis=0, tiled=True)
-    whole = lax.all_gather(own_rows, "sp", axis=0, tiled=True)
+    whole = gather_rows(own_rows, lax.axis_size("sp"))
     out_rows = lax.all_gather(w_output, "sp", axis=0, tiled=True)
+    whole, out_rows = lax.optimization_barrier((whole, out_rows))
     out_weight = lax.all_gather(out_rows, "dp", axis=1, tiled=True)
     head_out = attend(whole, columns, qk_gain, decay_sums[0])
     merged = lax.all_to_all(head_out, "sp", split_axis=0, concat_axis=1, tiled=True)

time: 291 us -> 201 us (0.69)
  the two profiles are of different devices: /device:TPU:29 before, /device:TPU:0 now
where the time goes in v2:
time: 201 us; the launch traced here: 200 us
  Pallas kernels  152 us (76%)
  blocking collectives  21.4 us (11%)
  between operations  13.2 us (7%)
  local copies, waits for them, and re-layouts  6.69 us (3%)
  matrix products  4.77 us (2%)
    pallas_call x1, Pallas kernels, gather_rows(): pl.pallas_call(functools.partial(ring_kernel, count), out_shape=jax.Shape...  117 us
    pallas_call x1, Pallas kernels, attend(): pl.pallas_call(functools.partial(attention_kernel, heads, width, block),...  35 us
    all_to_all x1, blocking collectives, on_device(): lax.all_to_all(head_out, 'sp', split_axis=0, concat_axis=1, tiled=True)  21.4 us
    unnamed x10, local copies, waits for them, and re-layouts  6.69 us
    dot_general x1, matrix products, on_device(): result = jnp.dot(merged, out_weight, preferred_element_type=jnp.float32)  4.77 us
  transfers between devices with their start and end apart: 3, of which 0 were waited for; matrix products, arithmetic and copies ran while one was open for 1% of the time, Pallas kernels for 76%

profile of v2, /device:TPU:0, one launch (start us, length us, event | category | flops | bytes accessed | tf_op | source)
XLA Modules:
  0.0 200.3 jit_solution(17895980241936103549)
XLA Ops:
  6.5 0.0 all-gather.4.cloned.1.call-start
  6.5 0.7 all-gather.4.cloned.1.call-update
  7.3 0.0 all-gather.6.cloned.1.call-start
  7.3 1.8 pad_maximum_fusion
  9.1 0.0 all-gather.6.cloned.1.call-update
  9.2 0.0 all-gather.8.cloned.1.call-start
  9.2 0.0 copy-start.1
  9.2 1.3 copy-done.1
  10.5 0.0 copy-start.2
  10.5 0.0 copy-start.3
  10.5 116.6 %shard_map.73.rows_ref = bf16[2560,2048]{1,0:T(8,128)(2,1)S(1)} custom-call(bf16[320,2048]{1,0:T(8,128)(2,1)S(1)} %bitcast.15), custom_call_target="tpu_custom_call" | custom-call | flops 99999997952 | bytes 10485760 | tf_op jit(solution)/shard_map/pallas_call | solution.py:189
  127.2 0.0 copy-start.4
  127.2 4.0 %copy-done.4 = bf16[2560,2048]{1,0:T(8,128)(2,1)} copy-done((bf16[2560,2048]{1,0:T(8,128)(2,1)}, bf16[2560,2048]{1,0:T(8,128)(2,1)S(1)}, u32[]{:S(2)}) %copy-start.4) | copy-done | bytes 10485784
  131.2 0.0 all-gather.4.cloned.1.call-done
  131.2 0.0 all-gather.8.cloned.1.call-update
  131.2 0.0 all-gather.6.cloned.1.call-done.weight_ref
  131.2 0.0 copy-done.2
  131.2 0.0 copy-done.3
  131.2 0.0 copy-start
  131.2 1.4 copy-done
  132.6 35.0 %shard_map.74 = bf16[2560,128]{1,0:T(8,128)(2,1)S(1)} custom-call(bf16[2560,2048]{1,0:T(8,128)(2,1)} %copy-done.4, bf16[2048,384]{1,0:T(8,128)(2,1)S(1)} %copy-done, f32[2,64]{1,0:T(2,128)S(1)} %copy-done.3, f32[2,2560]{1,0:T(2,128)S(1)} %bitcast.16), custom_call_target="tpu_custom_call" | custom-call | flops 7381975040 | bytes 10485760 | tf_op jit(solution)/shard_map/pallas_call | solution.py:102
  167.7 21.4 %all_to_all.19 = bf16[8,320,128]{2,1,0:T(8,128)(2,1)S(1)} all-to-all(bf16[8,320,128]{2,1,0:T(8,128)(2,1)S(1)} %bitcast.14), channel_id=1, replica_groups=mesh['sp'=8,'dp'=4] {'sp'}, dimensions={0} | all-to-all | bytes 1310720 | tf_op jit(solution)/shard_map/all_to_all | solution.py:217
  189.0 0.0 all-gather.8.cloned.1.call-done
  189.0 4.8 %fusion = bf16[1,320,2048]{2,1,0:T(8,128)(2,1)} fusion(bf16[1024,2048]{1,0:T(8,128)(2,1)} %all-gather.8.cloned.1.call-done, bf16[8,320,128]{2,1,0:T(8,128)(2,1)S(1)} %all_to_all.19), kind=kOutput, calls=%fused_computation.1 | convolution fusion | flops 1342832640 | bytes 6160384 | tf_op jit(solution)/shard_map/dot_general | solution.py:218
Async XLA Ops:
  6.5 124.6 %all-gather.4.cloned.1.call-start = ((), (), s32[]{:S(2)}) async-start(), calls=%async_computation.1 | async-start | bytes 1179648 | tf_op jit(solution)/shard_map/all_gather | solution.py:213
  7.3 123.9 %all-gather.6.cloned.1.call-start = ((), (), s32[]{:S(2)}) async-start(), calls=%async_computation.2 | async-start | bytes 1966080 | tf_op jit(solution)/shard_map/all_gather | solution.py:211
  9.2 179.9 %all-gather.8.cloned.1.call-start = ((), (), s32[]{:S(2)}) async-start(), calls=%async_computation.3 | async-start | bytes 5242880 | tf_op jit(solution)/shard_map/all_gather | solution.py:215
  9.2 1.3 copy-start.1
  10.5 120.7 %copy-start.2 = (f32[1,2,2560]{2,1,0:T(2,128)S(1)}, f32[1,2,2560]{2,1,0:T(2,128)}, u32[]{:S(2)}) copy-start(f32[1,2,2560]{2,1,0:T(2,128)} %param.13) | copy-start | bytes 61444
  10.5 120.7 %copy-start.3 = (f32[2,64]{1,0:T(2,128)S(1)}, f32[2,64]{1,0:T(2,128)}, u32[]{:S(2)}) copy-start(f32[2,64]{1,0:T(2,128)} %gain_ref.1) | copy-start | bytes 1540
  127.2 4.0 %copy-start.4 = (bf16[2560,2048]{1,0:T(8,128)(2,1)}, bf16[2560,2048]{1,0:T(8,128)(2,1)S(1)}, u32[]{:S(2)}) copy-start(bf16[2560,2048]{1,0:T(8,128)(2,1)S(1)} %shard_map.73.rows_ref) | copy-start | bytes 31457284
  131.2 1.4 copy-start
Sparse Core Ops, SparseCore 0:
  9.5 49.6 all-gather.3
  60.7 20.7 all-gather.5
  131.3 34.5 all-gather.7

commit v3 on v2

--- a/solution.py
+++ b/solution.py
@@ -12,9 +12,39 @@
 
 
 def attention_kernel(
-    heads, width, block, rows_ref, weight_ref, gain_ref, decay_ref, out_ref, key_ref, value_ref
+    heads,
+    width,
+    block,
+    count,
+    rows_ref,
+    weight_ref,
+    gain_ref,
+    decay_ref,
+    merged_ref,
+    key_ref,
+    value_ref,
+    done_ref,
+    send_sem,
+    recv_sem,
+    local_sem,
 ):
     index = pl.program_id(0)
+    me = lax.axis_index("sp")
+    rows = merged_ref.shape[1]
+    owners = block // rows
+
+    @pl.when(index == 0)
+    def _():
+        barrier = pltpu.get_barrier_semaphore()
+        for shift in range(1, count):
+            pl.semaphore_signal(
+                barrier,
+                inc=1,
+                device_id={"sp": lax.rem(me + shift, count)},
+                device_id_type=pl.DeviceIdType.MESH,
+            )
+        pl.semaphore_wait(barrier, count - 1)
+
     wide = heads * width
     place = pl.ds(pl.multiple_of(index * block, block), block)
     projected = jnp.dot(
@@ -89,32 +119,73 @@
         mixed, norm = total[:width], total[width : width + 1]
         scale = lax.rsqrt(jnp.mean(mixed * mixed, axis=0, keepdims=True) + EPS * norm * norm)
         outs.append(mixed * scale)
-    out_ref[...] = jnp.concatenate(outs, axis=0).T.astype(jnp.bfloat16)
-
-
-def attend(whole, weights, qk_gain, decay_rows):
+    turned = jnp.concatenate(outs, axis=0).T.astype(jnp.bfloat16)
+    for part in range(owners):
+        done_ref[index * owners + part] = turned[part * rows : (part + 1) * rows]
+
+    def remote(source, owner):
+        return pltpu.make_async_remote_copy(
+            src_ref=done_ref.at[owner],
+            dst_ref=merged_ref.at[source],
+            send_sem=send_sem.at[owner],
+            recv_sem=recv_sem.at[source],
+            device_id={"sp": owner},
+            device_id_type=pl.DeviceIdType.MESH,
+        )
+
+    def local():
+        return pltpu.make_async_copy(done_ref.at[me], merged_ref.at[me], local_sem)
+
+    for part in range(owners):
+        owner = index * owners + part
+
+        @pl.when(owner != me)
+        def _():
+            remote(me, owner).start()
+
+        @pl.when(owner == me)
+        def _():
+            local().start()
+
+    @pl.when(index == pl.num_programs(0) - 1)
+    def _():
+        for shift in range(1, count):
+            other = lax.rem(me + shift, count)
+            remote(other, other).wait_recv()
+            remote(me, other).wait_send()
+        local().wait()
+
+
+def attend(whole, weights, qk_gain, decay_rows, rows):
     length, depth = whole.shape
     heads = decay_rows.shape[0]
     width = qk_gain.shape[1]
-    block = 512
+    block = 2 * rows
     steps = length // block
+    count = length // rows
     wide = heads * width
     return pl.pallas_call(
-        functools.partial(attention_kernel, heads, width, block),
+        functools.partial(attention_kernel, heads, width, block, count),
         grid=(steps,),
-        out_shape=jax.ShapeDtypeStruct((length, wide), jnp.bfloat16),
+        out_shape=jax.ShapeDtypeStruct((count, rows, wide), jnp.bfloat16),
         in_specs=[
             pl.BlockSpec(memory_space=pltpu.VMEM),
             pl.BlockSpec((depth, 3 * wide), lambda i: (0, 0)),
             pl.BlockSpec((2, width), lambda i: (0, 0)),
             pl.BlockSpec((heads, block), lambda i: (0, i)),
         ],
-        out_specs=pl.BlockSpec((block, wide), lambda i: (i, 0)),
+        out_specs=pl.BlockSpec(memory_space=pl.ANY),
         scratch_shapes=[
             pltpu.VMEM((heads, length, 2 * width), jnp.bfloat16),
             pltpu.VMEM((heads, steps, width + 16, block), jnp.bfloat16),
+            pltpu.VMEM((count, rows, wide), jnp.bfloat16),
+            pltpu.SemaphoreType.DMA((count,)),
+            pltpu.SemaphoreType.DMA((count,)),
+            pltpu.SemaphoreType.DMA,
         ],
-        compiler_params=pltpu.CompilerParams(vmem_limit_bytes=44 * 1024 * 1024),
+        compiler_params=pltpu.CompilerParams(
+            collective_id=1, has_side_effects=True, vmem_limit_bytes=40 * 1024 * 1024
+        ),
         cost_estimate=pl.CostEstimate(
             flops=2 * length * depth * 3 * wide + 2 * heads * length * length * 2 * width,
             bytes_accessed=2 * length * depth,
@@ -126,7 +197,7 @@
 PIECES = 2
 
 
-def ring_kernel(count, own_ref, whole_ref, send_sem, recv_sem, local_sem):
+def ring_kernel(count, own_ref, whole_ref, mark_ref, send_sem, recv_sem, local_sem):
     rows = own_ref.shape[0]
     part = rows // (2 * PIECES)
     tall = 4 if count % 4 == 0 else 1
@@ -181,6 +252,7 @@
     for copy in copies.values():
         copy.wait_send()
     local.wait()
+    mark_ref[...] = jnp.zeros_like(mark_ref)
 
 
 def gather_rows(own_rows, count):
@@ -188,9 +260,12 @@
     shape = (count - 1, PIECES, 2)
     return pl.pallas_call(
         functools.partial(ring_kernel, count),
-        out_shape=jax.ShapeDtypeStruct((count * rows, depth), own_rows.dtype),
+        out_shape=(
+            jax.ShapeDtypeStruct((count * rows, depth), own_rows.dtype),
+            jax.ShapeDtypeStruct((8, 128), jnp.float32),
+        ),
         in_specs=[pl.BlockSpec(memory_space=pltpu.VMEM)],
-        out_specs=pl.BlockSpec(memory_space=pl.ANY),
+        out_specs=(pl.BlockSpec(memory_space=pl.ANY), pl.BlockSpec(memory_space=pltpu.VMEM)),
         scratch_shapes=[
             pltpu.SemaphoreType.DMA(shape),
             pltpu.SemaphoreType.DMA(shape),
@@ -209,12 +284,12 @@
     own_rows = tokens[0]
     stacked = jnp.concatenate((w_query, w_key, w_value), axis=1)
     columns = lax.all_gather(stacked, "dp", axis=0, tiled=True)
-    whole = gather_rows(own_rows, lax.axis_size("sp"))
+    whole, mark = gather_rows(own_rows, lax.axis_size("sp"))
     out_rows = lax.all_gather(w_output, "sp", axis=0, tiled=True)
-    whole, out_rows = lax.optimization_barrier((whole, out_rows))
+    mark, out_rows = lax.optimization_barrier((mark, out_rows))
     out_weight = lax.all_gather(out_rows, "dp", axis=1, tiled=True)
-    head_out = attend(whole, columns, qk_gain, decay_sums[0])
-    merged = lax.all_to_all(head_out, "sp", split_axis=0, concat_axis=1, tiled=True)
+    merged = attend(whole, columns, qk_gain, decay_sums[0], own_rows.shape[0])
+    merged = merged.transpose(1, 0, 2).reshape(own_rows.shape[0], -1)
     result = jnp.dot(merged, out_weight, preferred_element_type=jnp.float32)
     return result.astype(jnp.bfloat16)[None]
 

time: 201 us -> 213 us (1.060)
  the two profiles are of different devices: /device:TPU:0 before, /device:TPU:29 now
where the time goes in v3:
time: 213 us
  Pallas kernels  144 us (68%)
  waiting for transfers between devices  38.2 us (18%)
  between operations  13.2 us (6%)
  local copies, waits for them, and re-layouts  10.7 us (5%)
  matrix products  4.82 us (2%)
    pallas_call x1, Pallas kernels, gather_rows(): pl.pallas_call(functools.partial(ring_kernel, count), out_shape=(jax.Shap...  101 us
    pallas_call x1, Pallas kernels, attend(): pl.pallas_call(functools.partial(attention_kernel, heads, width, block, c...  43.2 us
    all_gather x1, waiting for transfers between devices, on_device(): out_rows = lax.all_gather(w_output, 'sp', axis=0, tiled=True)  37.4 us
    unnamed x12, local copies, waits for them, and re-layouts  10.7 us
    dot_general x1, matrix products, on_device(): result = jnp.dot(merged, out_weight, preferred_element_type=jnp.float32)  4.82 us
  transfers between devices with their start and end apart: 3, of which 1 were waited for; matrix products, arithmetic and copies ran while one was open for 1% of the time, Pallas kernels for 68%

profile of v3, /device:TPU:29, one launch (start us, length us, event | category | flops | bytes accessed | tf_op | source)
XLA Modules:
  0.0 212.6 jit_solution(5904051450407129753)
XLA Ops:
  6.5 0.0 all-gather.6.cloned.1.call-start
  6.5 0.7 all-gather.6.cloned.1.call-update
  7.3 0.0 all-gather.4.cloned.1.call-start
  7.3 1.8 pad_maximum_fusion
  9.1 0.0 all-gather.4.cloned.1.call-update
  9.2 0.0 all-gather.8.cloned.1.call-start
  9.2 37.4 %all-gather.6.cloned.1.call-done = bf16[1024,512]{1,0:T(8,128)(2,1)} async-done(((bf16[128,512]{1,0:T(8,128)(2,1)}), bf16[1024,512]{1,0:T(8,128)(2,1)}) %all-gather.6.cloned.1.call-update) | async-done | bytes 1048592 | tf_op jit(solution)/shard_map/all_gather | solution.py:288
  46.6 0.0 all-gather.8.cloned.1.call-update
  46.6 0.0 copy-start.1
  46.7 1.3 copy-done.1
  48.0 0.0 copy-start.2
  48.0 0.0 copy-start.3
  48.0 100.7 %shard_map.73 = (bf16[2560,2048]{1,0:T(8,128)(2,1)S(1)}, f32[8,128]{1,0:T(8,128)}) custom-call(bf16[320,2048]{1,0:T(8,128)(2,1)S(1)} %bitcast.13), custom_call_target="tpu_custom_call" | custom-call | flops 99999997952 | bytes 10485760 | tf_op jit(solution)/shard_map/pallas_call | solution.py:261
  148.6 0.0 copy-start.4
  148.6 4.0 %copy-done.4 = bf16[2560,2048]{1,0:T(8,128)(2,1)} copy-done((bf16[2560,2048]{1,0:T(8,128)(2,1)}, bf16[2560,2048]{1,0:T(8,128)(2,1)S(1)}, u32[]{:S(2)}) %copy-start.4) | copy-done | bytes 10485784
  152.6 0.0 all-gather.4.cloned.1.call-done.weight_ref
  152.6 0.0 copy-done.2
  152.6 0.0 copy-done.3
  152.6 0.0 copy-start
  152.6 1.4 copy-done
  154.0 0.0 copy-start.5
  154.0 4.0 %copy-done.5 = bf16[2560,2048]{1,0:T(8,128)(2,1)S(1)} copy-done((bf16[2560,2048]{1,0:T(8,128)(2,1)S(1)}, bf16[2560,2048]{1,0:T(8,128)(2,1)}, u32[]{:S(2)}) %copy-start.5) | copy-done | bytes 10485784
  158.0 43.2 %shard_map.74 = bf16[8,320,128]{2,1,0:T(8,128)(2,1)S(1)} custom-call(bf16[2560,2048]{1,0:T(8,128)(2,1)S(1)} %copy-done.5, bf16[2048,384]{1,0:T(8,128)(2,1)S(1)} %copy-done, f32[2,64]{1,0:T(2,128)S(1)} %copy-done.3, f32[2,2560]{1,0:T(2,128)S(1)} %bitcast.14), custom_call_target="tpu_custom_call" | custom-call | flops 7381975040 | bytes 10485760 | tf_op jit(solution)/shard_map/pallas_call | solution.py:167
  201.2 0.0 all-gather.8.cloned.1.call-done
  201.3 4.8 %fusion = bf16[1,320,2048]{2,1,0:T(8,128)(2,1)} fusion(bf16[1024,2048]{1,0:T(8,128)(2,1)} %all-gather.8.cloned.1.call-done, bf16[8,320,128]{2,1,0:T(8,128)(2,1)S(1)} %shard_map.74), kind=kOutput, calls=%fused_computation.1 | convolution fusion | flops 1342832640 | bytes 6160384 | tf_op jit(solution)/shard_map/dot_general | solution.py:293
Async XLA Ops:
  6.5 40.1 %all-gather.6.cloned.1.call-start = ((), (), s32[]{:S(2)}) async-start(), calls=%async_computation.1 | async-start | bytes 1179648 | tf_op jit(solution)/shard_map/all_gather | solution.py:288
  7.3 145.4 %all-gather.4.cloned.1.call-start = ((), (), s32[]{:S(2)}) async-start(), calls=%async_computation | async-start | bytes 1966080 | tf_op jit(solution)/shard_map/all_gather | solution.py:286
  9.2 192.1 %all-gather.8.cloned.1.call-start = ((), (), s32[]{:S(2)}) async-start(), calls=%async_computation.2 | async-start | bytes 5242880 | tf_op jit(solution)/shard_map/all_gather | solution.py:290
  46.6 1.3 copy-start.1
  48.0 104.7 %copy-start.2 = (f32[1,2,2560]{2,1,0:T(2,128)S(1)}, f32[1,2,2560]{2,1,0:T(2,128)}, u32[]{:S(2)}) copy-start(f32[1,2,2560]{2,1,0:T(2,128)} %param.13) | copy-start | bytes 61444
  48.0 104.7 %copy-start.3 = (f32[2,64]{1,0:T(2,128)S(1)}, f32[2,64]{1,0:T(2,128)}, u32[]{:S(2)}) copy-start(f32[2,64]{1,0:T(2,128)} %gain_ref.1) | copy-start | bytes 1540
  148.6 4.0 %copy-start.4 = (bf16[2560,2048]{1,0:T(8,128)(2,1)}, bf16[2560,2048]{1,0:T(8,128)(2,1)S(1)}, u32[]{:S(2)}) copy-start(bf16[2560,2048]{1,0:T(8,128)(2,1)S(1)} %get-tuple-element.6.rows_ref) | copy-start | bytes 31457284
  152.6 1.4 copy-start
  154.0 4.0 %copy-start.5 = (bf16[2560,2048]{1,0:T(8,128)(2,1)S(1)}, bf16[2560,2048]{1,0:T(8,128)(2,1)}, u32[]{:S(2)}) copy-start(bf16[2560,2048]{1,0:T(8,128)(2,1)} %copy-done.4) | copy-start | bytes 31457284
Sparse Core Ops, SparseCore 0:
  9.5 37.1 all-gather.5
  48.2 22.7 all-gather.3
  72.6 34.4 all-gather.7

commit v4 on v3

--- a/solution.py
+++ b/solution.py
@@ -48,7 +48,7 @@
     wide = heads * width
     place = pl.ds(pl.multiple_of(index * block, block), block)
     projected = jnp.dot(
-        rows_ref[place, :], weight_ref[...], preferred_element_type=jnp.float32
+        rows_ref[...], weight_ref[...], preferred_element_type=jnp.float32
     ).astype(jnp.bfloat16)
 
     def unit(values, gain):
@@ -169,7 +169,7 @@
         grid=(steps,),
         out_shape=jax.ShapeDtypeStruct((count, rows, wide), jnp.bfloat16),
         in_specs=[
-            pl.BlockSpec(memory_space=pltpu.VMEM),
+            pl.BlockSpec((block, depth), lambda i: (i, 0)),
             pl.BlockSpec((depth, 3 * wide), lambda i: (0, 0)),
             pl.BlockSpec((2, width), lambda i: (0, 0)),
             pl.BlockSpec((heads, block), lambda i: (0, i)),
@@ -197,7 +197,9 @@
 PIECES = 2
 
 
-def ring_kernel(count, own_ref, whole_ref, mark_ref, send_sem, recv_sem, local_sem):
+def ring_kernel(
+    count, own_ref, slab_ref, whole_ref, slabs_ref, send_sem, recv_sem, slab_send, slab_recv, local_sem
+):
     rows = own_ref.shape[0]
     part = rows // (2 * PIECES)
     tall = 4 if count % 4 == 0 else 1
@@ -223,9 +225,17 @@
     pl.semaphore_wait(barrier, 2)
 
     local = pltpu.make_async_copy(
-        own_ref, whole_ref.at[pl.ds(pl.multiple_of(me * rows, rows), rows)], local_sem
+        own_ref, whole_ref.at[pl.ds(pl.multiple_of(me * rows, rows), rows)], local_sem.at[0]
     )
     local.start()
+    tall_slab = slab_ref.shape[0]
+    half = tall_slab // 2
+    local_slab = pltpu.make_async_copy(
+        slab_ref,
+        slabs_ref.at[pl.ds(pl.multiple_of(me * tall_slab, tall_slab), tall_slab)],
+        local_sem.at[1],
+    )
+    local_slab.start()
     copies = {}
     for step in range(count - 1):
         for piece in range(PIECES):
@@ -246,30 +256,48 @@
                 )
                 copy.start()
                 copies[step, piece, side] = copy
-    for piece in range(PIECES):
+        for side, way in enumerate(ways):
+            if step:
+                copies[step - 1, "slab", side].wait_recv()
+            origin = member(spot - way * step)
+            place = pl.ds(pl.multiple_of(origin * tall_slab + side * half, half), half)
+            source = slab_ref.at[pl.ds(side * half, half)] if step == 0 else slabs_ref.at[place]
+            copy = pltpu.make_async_remote_copy(
+                src_ref=source,
+                dst_ref=slabs_ref.at[place],
+                send_sem=slab_send.at[step, side],
+                recv_sem=slab_recv.at[step, side],
+                device_id={"sp": targets[side]},
+                device_id_type=pl.DeviceIdType.MESH,
+            )
+            copy.start()
+            copies[step, "slab", side] = copy
+    for piece in (*range(PIECES), "slab"):
         for side in range(2):
             copies[count - 2, piece, side].wait_recv()
     for copy in copies.values():
         copy.wait_send()
     local.wait()
-    mark_ref[...] = jnp.zeros_like(mark_ref)
-
-
-def gather_rows(own_rows, count):
+    local_slab.wait()
+
+
+def gather_rows(own_rows, slab, count):
     rows, depth = own_rows.shape
     shape = (count - 1, PIECES, 2)
     return pl.pallas_call(
         functools.partial(ring_kernel, count),
         out_shape=(
             jax.ShapeDtypeStruct((count * rows, depth), own_rows.dtype),
-            jax.ShapeDtypeStruct((8, 128), jnp.float32),
-        ),
-        in_specs=[pl.BlockSpec(memory_space=pltpu.VMEM)],
-        out_specs=(pl.BlockSpec(memory_space=pl.ANY), pl.BlockSpec(memory_space=pltpu.VMEM)),
+            jax.ShapeDtypeStruct((count * slab.shape[0], slab.shape[1]), slab.dtype),
+        ),
+        in_specs=[pl.BlockSpec(memory_space=pltpu.VMEM)] * 2,
+        out_specs=(pl.BlockSpec(memory_space=pltpu.HBM), pl.BlockSpec(memory_space=pltpu.HBM)),
         scratch_shapes=[
             pltpu.SemaphoreType.DMA(shape),
             pltpu.SemaphoreType.DMA(shape),
-            pltpu.SemaphoreType.DMA,
+            pltpu.SemaphoreType.DMA((count - 1, 2)),
+            pltpu.SemaphoreType.DMA((count - 1, 2)),
+            pltpu.SemaphoreType.DMA((2,)),
         ],
         compiler_params=pltpu.CompilerParams(
             collective_id=0, has_side_effects=True, vmem_limit_bytes=16 * 1024 * 1024
@@ -277,16 +305,14 @@
         cost_estimate=pl.CostEstimate(
             flops=10**11, bytes_accessed=2 * count * rows * depth, transcendentals=0
         ),
-    )(own_rows)
+    )(own_rows, slab)
 
 
 def on_device(tokens, w_query, w_key, w_value, w_output, qk_gain, decay_sums):
     own_rows = tokens[0]
     stacked = jnp.concatenate((w_query, w_key, w_value), axis=1)
     columns = lax.all_gather(stacked, "dp", axis=0, tiled=True)
-    whole, mark = gather_rows(own_rows, lax.axis_size("sp"))
-    out_rows = lax.all_gather(w_output, "sp", axis=0, tiled=True)
-    mark, out_rows = lax.optimization_barrier((mark, out_rows))
+    whole, out_rows = gather_rows(own_rows, w_output, lax.axis_size("sp"))
     out_weight = lax.all_gather(out_rows, "dp", axis=1, tiled=True)
     merged = attend(whole, columns, qk_gain, decay_sums[0], own_rows.shape[0])
     merged = merged.transpose(1, 0, 2).reshape(own_rows.shape[0], -1)

time: 213 us -> 185 us (0.87)
  waiting for transfers between devices: 38.2 us -> 0.07 us
  Pallas kernels: 144 us -> 152 us
    all_gather x1 -> x0, waiting for transfers between devices: 37.4 us -> none  [on_device(): out_rows = lax.all_gather(w_output, 'sp', axis=0, tiled=True)]
    pallas_call x1, Pallas kernels: 101 us -> 111 us  [gather_rows(): pl.pallas_call(functools.partial(ring_kernel, count), out_shape=(jax.Shap...]
    unnamed x12 -> x14, local copies, waits for them, and re-layouts: 10.7 us -> 11.6 us
  transfers between devices with their start and end apart: 3 -> 2, of which waited for: 1 -> 0; matrix products, arithmetic and copies ran while one was open for 1% -> 0% of each run, Pallas kernels for 68% -> 83%
where the time goes in v4:
time: 185 us; the launch traced here: 184 us
  Pallas kernels  152 us (82%)
  between operations  13.5 us (7%)
  local copies, waits for them, and re-layouts  11.6 us (6%)
  matrix products  4.83 us (3%)
    pallas_call x1, Pallas kernels, gather_rows(): pl.pallas_call(functools.partial(ring_kernel, count), out_shape=(jax.Shap...  111 us
    pallas_call x1, Pallas kernels, attend(): pl.pallas_call(functools.partial(attention_kernel, heads, width, block, c...  41.6 us
    unnamed x14, local copies, waits for them, and re-layouts  11.6 us
    dot_general x1, matrix products, on_device(): result = jnp.dot(merged, out_weight, preferred_element_type=jnp.float32)  4.83 us
  transfers between devices with their start and end apart: 2, of which 0 were waited for; matrix products, arithmetic and copies ran while one was open for 0% of the time, Pallas kernels for 83%

profile of v4, /device:TPU:29, one launch (start us, length us, event | category | flops | bytes accessed | tf_op | source)
XLA Modules:
  0.0 184.0 jit_solution(6267713526737100647)
XLA Ops:
  6.5 0.0 all-gather.3.cloned.1.call-start
  6.5 1.8 pad_maximum_fusion
  8.4 0.0 all-gather.3.cloned.1.call-update
  8.4 0.0 all-gather.5.cloned.1.call-start
  8.4 0.0 copy-start.1
  8.5 1.3 copy-done.1
  9.8 0.0 copy-start.2
  9.8 0.9 copy-done.2
  10.7 0.0 copy-start.3
  10.7 0.0 copy-start.4
  10.7 110.7 %shard_map.73 = (bf16[2560,2048]{1,0:T(8,128)(2,1)S(1)}, bf16[1024,512]{1,0:T(8,128)(2,1)}) custom-call(bf16[320,2048]{1,0:T(8,128)(2,1)S(1)} %bitcast.13, bf16[128,512]{1,0:T(8,128)(2,1)S(1)} %copy-done.2), custom_call_target="tpu_custom_call" | custom-call | flops 99999997952 | bytes 10485760 | tf_op jit(solution)/shard_map/pallas_call | solution.py:287
  121.3 0.0 copy-start.5
  121.3 4.0 %copy-done.5 = bf16[2560,2048]{1,0:T(8,128)(2,1)} copy-done((bf16[2560,2048]{1,0:T(8,128)(2,1)}, bf16[2560,2048]{1,0:T(8,128)(2,1)S(1)}, u32[]{:S(2)}) %copy-start.5) | copy-done | bytes 10485784
  125.3 0.0 all-gather.5.cloned.1.call-update
  125.3 0.0 all-gather.3.cloned.1.call-done.weight_ref
  125.4 0.0 copy-done.3
  125.4 0.0 copy-done.4
  125.4 0.0 copy-start
  125.4 1.4 copy-done
  126.8 0.0 copy-start.6
  126.8 4.0 %copy-done.6 = bf16[2560,2048]{1,0:T(8,128)(2,1)S(1)} copy-done((bf16[2560,2048]{1,0:T(8,128)(2,1)S(1)}, bf16[2560,2048]{1,0:T(8,128)(2,1)}, u32[]{:S(2)}) %copy-start.6) | copy-done | bytes 10485784
  130.8 41.6 %shard_map.74 = bf16[8,320,128]{2,1,0:T(8,128)(2,1)S(1)} custom-call(bf16[2560,2048]{1,0:T(8,128)(2,1)S(1)} %copy-done.6, bf16[2048,384]{1,0:T(8,128)(2,1)S(1)} %copy-done, f32[2,64]{1,0:T(2,128)S(1)} %copy-done.4, f32[2,2560]{1,0:T(2,128)S(1)} %bitcast.14), custom_call_target="tpu_custom_call" | custom-call | flops 7381975040 | bytes 10485760 | tf_op jit(solution)/shard_map/pallas_call | solution.py:167
  172.3 0.0 all-gather.5.cloned.1.call-done
  172.4 4.8 %fusion = bf16[1,320,2048]{2,1,0:T(8,128)(2,1)} fusion(bf16[1024,2048]{1,0:T(8,128)(2,1)} %all-gather.5.cloned.1.call-done, bf16[8,320,128]{2,1,0:T(8,128)(2,1)S(1)} %shard_map.74), kind=kOutput, calls=%fused_computation.1 | convolution fusion | flops 1342832640 | bytes 6160384 | tf_op jit(solution)/shard_map/dot_general | solution.py:319
Async XLA Ops:
  6.5 118.8 %all-gather.3.cloned.1.call-start = ((), (), s32[]{:S(2)}) async-start(), calls=%async_computation | async-start | bytes 1966080 | tf_op jit(solution)/shard_map/all_gather | solution.py:314
  8.4 164.0 %all-gather.5.cloned.1.call-start = ((), (), s32[]{:S(2)}) async-start(), calls=%async_computation.1 | async-start | bytes 5242880 | tf_op jit(solution)/shard_map/all_gather | solution.py:316
  8.4 1.3 copy-start.1
  9.8 0.9 copy-start.2
  10.7 114.7 %copy-start.3 = (f32[1,2,2560]{2,1,0:T(2,128)S(1)}, f32[1,2,2560]{2,1,0:T(2,128)}, u32[]{:S(2)}) copy-start(f32[1,2,2560]{2,1,0:T(2,128)} %param.13) | copy-start | bytes 61444
  10.7 114.7 %copy-start.4 = (f32[2,64]{1,0:T(2,128)S(1)}, f32[2,64]{1,0:T(2,128)}, u32[]{:S(2)}) copy-start(f32[2,64]{1,0:T(2,128)} %gain_ref.1) | copy-start | bytes 1540
  121.3 4.0 %copy-start.5 = (bf16[2560,2048]{1,0:T(8,128)(2,1)}, bf16[2560,2048]{1,0:T(8,128)(2,1)S(1)}, u32[]{:S(2)}) copy-start(bf16[2560,2048]{1,0:T(8,128)(2,1)S(1)} %get-tuple-element.7.rows_ref) | copy-start | bytes 31457284
  125.4 1.4 copy-start
  126.8 4.0 %copy-start.6 = (bf16[2560,2048]{1,0:T(8,128)(2,1)S(1)}, bf16[2560,2048]{1,0:T(8,128)(2,1)}, u32[]{:S(2)}) copy-start(bf16[2560,2048]{1,0:T(8,128)(2,1)} %copy-done.5) | copy-start | bytes 31457284
Sparse Core Ops, SparseCore 0:
  8.9 20.9 all-gather.2
  125.5 36.7 all-gather.4

commit v5 on v0

v5 whole, which is shorter than its diff:
```python
import functools

import jax
import jax.numpy as jnp
from jax import lax
from jax.experimental import pallas as pl
from jax.experimental.pallas import tpu as pltpu
from jax.sharding import PartitionSpec as P

EPS = 1e-06
DIMS_NT = (((1,), (1,)), ((), ()))


PIECES = 2
MESH = pl.DeviceIdType.MESH


def layer_kernel(
    heads, width, count, groups,
    own_ref, stacked_ref, slab_ref, gain_ref, decay_ref, out_ref,
    whole_ref, weight_ref, slabs_ref, projected_ref, key_ref, value_ref, done_ref, merged_ref,
    send_sem, recv_sem, slab_send, slab_recv, pass_send, pass_recv, weight_send, weight_recv,
    done_send, done_recv,
):
    rows, depth = own_ref.shape
    owners = 2
    block = owners * rows
    wide = heads * width
    part = rows // (2 * PIECES)
    tall = 4 if count % 4 == 0 else 1
    broad = count // tall
    me, group = lax.axis_index("sp"), lax.axis_index("dp")

    def member(spot):
        spot = lax.rem(spot + 2 * count, count)
        column, height = spot // tall, lax.rem(spot, tall)
        level = height + lax.rem(column, 2) * (tall - 1 - 2 * height)
        return level * broad + column

    level, column = me // broad, lax.rem(me, broad)
    spot = column * tall + level + lax.rem(column, 2) * (tall - 1 - 2 * level)
    ways = (1, -1)
    targets = [member(spot + way) for way in ways]
    peers = [lax.rem(group + shift, groups) for shift in range(1, groups)]

    barrier = pltpu.get_barrier_semaphore()
    for shift in range(1, count):
        other = lax.rem(me + shift, count)
        pl.semaphore_signal(barrier, inc=1, device_id={"sp": other}, device_id_type=MESH)
    for peer in peers:
        pl.semaphore_signal(barrier, inc=1, device_id={"dp": peer}, device_id_type=MESH)
    pl.semaphore_wait(barrier, count + groups - 2)

    def send(source, target, out_sem, in_sem, device):
        copy = pltpu.make_async_remote_copy(
            src_ref=source, dst_ref=target, send_sem=out_sem, recv_sem=in_sem,
            device_id=device, device_id_type=MESH,
        )
        copy.start()
        return copy

    tall_slab = slab_ref.shape[0]
    half = tall_slab // 2
    copies, passed, weights, backlog = {}, [], [], []

    def slab_place(origin, side):
        return pl.ds(pl.multiple_of(origin * tall_slab + side * half, half), half)

    def pass_on(step, side, source, place):
        for number, peer in enumerate(peers):
            passed.append(
                send(
                    source, slabs_ref.at[group, place], pass_send.at[number, step, side],
                    pass_recv.at[number, step, side], {"dp": peer},
                )
            )

    def project(place):
        projected_ref[place, :] = jnp.dot(
            whole_ref[place, :], weight_ref[...].reshape(depth, 3 * wide),
            preferred_element_type=jnp.float32,
        ).astype(jnp.bfloat16)

    for step in range(count):
        arrived = []
        for piece in range(PIECES):
            for side, way in enumerate(ways):
                offset = (side * PIECES + piece) * part
                if step:
                    copies[step - 1, piece, side].wait_recv()
                if step == count - 1:
                    continue
                origin = member(spot - way * step)
                place = pl.ds(pl.multiple_of(origin * rows + offset, part), part)
                source = own_ref.at[pl.ds(offset, part)] if step == 0 else whole_ref.at[place]
                copies[step, piece, side] = send(
                    source, whole_ref.at[place], send_sem.at[step, piece, side],
                    recv_sem.at[step, piece, side], {"sp": targets[side]},
                )
        for side, way in enumerate(ways):
            if step:
                copies[step - 1, "slab", side].wait_recv()
            origin = member(spot - way * step)
            place = slab_place(origin, side)
            source = (
                slab_ref.at[pl.ds(side * half, half)]
                if step == 0
                else slabs_ref.at[group, place]
            )
            if step < count - 1:
                copies[step, "slab", side] = send(
                    source, slabs_ref.at[group, place], slab_send.at[step, side],
                    slab_recv.at[step, side], {"sp": targets[side]},
                )
            if step == 0:
                for number, peer in enumerate(peers if side == 0 else ()):
                    weights.append(
                        send(
                            stacked_ref, weight_ref.at[group], weight_send.at[number],
                            weight_recv.at[number], {"dp": peer},
                        )
                    )
            pass_on(step, side, source, place)
            start = origin * rows + side * PIECES * part
            backlog.append(pl.ds(pl.multiple_of(start, PIECES * part), PIECES * part))
        if step == 0:
            whole_ref[pl.ds(pl.multiple_of(me * rows, rows), rows), :] = own_ref[...]
            weight_ref[group] = stacked_ref[...]
            slabs_ref[group, pl.ds(pl.multiple_of(me * tall_slab, tall_slab), tall_slab), :] = (
                slab_ref[...]
            )
        if step == min(3, count - 1):
            for copy in weights:
                copy.wait_recv()
        if step >= min(3, count - 1):
            for place in backlog:
                project(place)
            backlog = []


    def remote(source, owner):
        return pltpu.make_async_remote_copy(
            src_ref=done_ref.at[owner], dst_ref=merged_ref.at[source],
            send_sem=done_send.at[owner], recv_sem=done_recv.at[source],
            device_id={"sp": owner}, device_id_type=MESH,
        )

    def one_block(index, unused):
        place = pl.ds(pl.multiple_of(index * block, block), block)
        projected = projected_ref[place, :]

        def unit(values, gain):
            values = values.astype(jnp.float32)
            scale = lax.rsqrt(jnp.mean(values * values, axis=-1, keepdims=True) + EPS)
            return values * scale * gain

        values_turned = projected[:, 2 * wide :].astype(jnp.float32).T
        lane = lax.broadcasted_iota(jnp.int32, (block, width), 1)
        ones_lanes = jnp.where(lane < 3, 1.0, 0.0)
        sub = lax.broadcasted_iota(jnp.int32, (2 * width, block), 0)
        ones_rows = jnp.where(
            lax.broadcasted_iota(jnp.int32, (16, block), 0) == 0, 1.0, 0.0
        )
        queries = []
        for head in range(heads):
            low = head * width
            query = unit(projected[:, low : low + width], gain_ref[0:1, :]) * width ** (-0.5)
            key = unit(projected[:, wide + low : wide + low + width], gain_ref[1:2, :])
            decay = -decay_ref[head : head + 1, place]
            first = decay.astype(jnp.bfloat16).astype(jnp.float32)
            rest = decay - first
            second = rest.astype(jnp.bfloat16).astype(jnp.float32)
            third = rest - second
            parts = jnp.where(
                sub == 0, first, jnp.where(sub == 1, second, jnp.where(sub == 2, third, 0.0))
            ).T
            queries.append(jnp.concatenate([query, ones_lanes], axis=1).astype(jnp.bfloat16))
            key_ref[head, place, :] = jnp.concatenate([key, parts[:, :width]], axis=1).astype(
                jnp.bfloat16
            )
            value_ref[head, index] = jnp.concatenate(
                [values_turned[low : low + width], ones_rows], axis=0
            ).astype(jnp.bfloat16)

        def step(column, carry, masked):
            fresh = []
            for head in range(heads):
                peak, total = carry[head]
                keys = key_ref[head, pl.ds(pl.multiple_of(column * block, block), block), :]
                scores = lax.dot_general(
                    keys, queries[head], DIMS_NT, preferred_element_type=jnp.float32
                )
                if masked:
                    key_place = lax.broadcasted_iota(jnp.int32, scores.shape, 0)
                    query_place = lax.broadcasted_iota(jnp.int32, scores.shape, 1)
                    scores = jnp.where(key_place <= query_place, scores, -jnp.inf)
                higher = jnp.maximum(peak, jnp.max(scores, axis=0, keepdims=True))
                probs = jnp.exp(scores - higher).astype(jnp.bfloat16)
                total = total * jnp.exp(peak - higher) + jnp.dot(
                    value_ref[head, column], probs, preferred_element_type=jnp.float32
                )
                fresh.append((higher, total))
            return tuple(fresh)

        start = tuple(
            (
                jnp.full((1, block), -1e30, jnp.float32),
                jnp.zeros((width + 16, block), jnp.float32),
            )
            for _ in range(heads)
        )
        carry = step(index, start, True)
        carry = lax.fori_loop(0, index, lambda column, c: step(column, c, False), carry)
        outs = []
        for head in range(heads):
            total = carry[head][1]
            mixed, norm = total[:width], total[width : width + 1]
            scale = lax.rsqrt(jnp.mean(mixed * mixed, axis=0, keepdims=True) + EPS * norm * norm)
            outs.append(mixed * scale)
        turned = jnp.concatenate(outs, axis=0).T.astype(jnp.bfloat16)
        for part_index in range(owners):
            owner = index * owners + part_index
            done_ref[owner] = turned[part_index * rows : (part_index + 1) * rows]

            @pl.when(owner != me)
            def _():
                remote(me, owner).start()

        return unused

    lax.fori_loop(0, count // owners, one_block, 0)
    merged_ref[me] = done_ref[me]
    for copy in passed:
        copy.wait_recv()
    for shift in range(1, count):
        other = lax.rem(me + shift, count)
        remote(other, other).wait_recv()
    merged = jnp.concatenate([merged_ref[source] for source in range(count)], axis=1)
    columns = slab_ref.shape[1]
    for place in range(groups):
        out_ref[:, place * columns : (place + 1) * columns] = jnp.dot(
            merged, slabs_ref[place], preferred_element_type=jnp.float32
        ).astype(out_ref.dtype)
    for copy in (*copies.values(), *passed, *weights):
        copy.wait_send()
    for shift in range(1, count):
        remote(me, lax.rem(me + shift, count)).wait_send()


def on_device(tokens, w_query, w_key, w_value, w_output, qk_gain, decay_sums):
    own_rows, decay_rows = tokens[0], decay_sums[0]
    count, groups = lax.axis_size("sp"), lax.axis_size("dp")
    rows, depth = own_rows.shape
    heads, width = decay_rows.shape[0], qk_gain.shape[1]
    wide, length, block = heads * width, count * rows, 2 * rows
    stacked = jnp.concatenate((w_query, w_key, w_value), axis=1)
    tall_slab, columns = w_output.shape
    bf16, sem = jnp.bfloat16, pltpu.SemaphoreType.DMA
    ring = (count - 1, PIECES, 2)
    result = pl.pallas_call(
        functools.partial(layer_kernel, heads, width, count, groups),
        out_shape=jax.ShapeDtypeStruct((rows, depth), bf16),
        in_specs=[pl.BlockSpec(memory_space=pltpu.VMEM)] * 5,
        out_specs=pl.BlockSpec(memory_space=pltpu.VMEM),
        scratch_shapes=[
            pltpu.VMEM((length, depth), bf16),
            pltpu.VMEM((groups, depth // groups, 3 * wide), bf16),
            pltpu.VMEM((groups, count * tall_slab, columns), bf16),
            pltpu.VMEM((length, 3 * wide), bf16),
            pltpu.VMEM((heads, length, 2 * width), bf16),
            pltpu.VMEM((heads, length // block, width + 16, block), bf16),
            pltpu.VMEM((count, rows, wide), bf16),
            pltpu.VMEM((count, rows, wide), bf16),
            sem(ring), sem(ring), sem((count - 1, 2)), sem((count - 1, 2)),
            sem((groups - 1, count, 2)), sem((groups - 1, count, 2)),
            sem((groups - 1,)), sem((groups - 1,)), sem((count,)), sem((count,)),
        ],
        compiler_params=pltpu.CompilerParams(
            collective_id=0, has_side_effects=True, vmem_limit_bytes=60 * 1024 * 1024
        ),
    )(own_rows, stacked, w_output, qk_gain, decay_rows)
    return result[None]


def solution(mesh):
    placed = (
        P("dp", "sp", None),
        P("dp", "sp"),
        P("dp", "sp"),
        P("dp", "sp"),
        P("sp", "dp"),
        P(),
        P("dp", "sp", None),
    )
    return jax.shard_map(
        on_device, mesh=mesh, in_specs=placed, out_specs=P("dp", "sp", None), check_vma=False
    )
```

time: 414 us -> 156 us (0.38); the launches traced: 409 us -> 156 us
  waiting for transfers between devices: 178 us -> 0 us
  Pallas kernels: 0 us -> 152 us
  other arithmetic: 75.1 us -> 1.83 us
  matrix products: 66.4 us -> 0 us
  local copies, waits for them, and re-layouts: 54.8 us -> 2.52 us
  between operations: 13.3 us -> 0.01 us
  blocking collectives: 8.13 us -> 0 us
  loops' own time: 7.36 us -> 0 us
  starting transfers between devices: 6.1 us -> 0 us
    all_gather x3 -> x0, waiting for transfers between devices: 162 us -> none  [the longest x1 150 us: on_device(): whole = lax.all_gather(own_rows, 'sp', axis=0, tiled=True)]
    pallas_call x0 -> x1, Pallas kernels: none -> 152 us  [on_device(): pl.pallas_call(functools.partial(layer_kernel, heads, width, count, group...]
    div x5 -> x0, other arithmetic: 69 us -> none  [one_block(): weights / jnp.sum(weights, axis=-1, keepdims=True)]
    dot_general x32 -> x0, matrix products: 66.4 us -> none  [the longest x15 29.8 us: fill(): jnp.einsum('qhd,khd->hqk', query_block, key_block, preferred_element_type...]
    another operation x10 -> x0, local copies, waits for them, and re-layouts: 26.7 us -> none
    dynamic_slice x30 -> x0, local copies, waits for them, and re-layouts: 16.8 us -> none  [the longest x15 10.3 us: fill(): decay_keys = lax.dynamic_slice_in_dim(decay_rows, key_start, block, 1)]
    all_to_all x1 -> x0, waiting for transfers between devices: 15.6 us -> none  [on_device(): lax.all_to_all(head_out, 'sp', split_axis=0, concat_axis=1, tiled=True)]
    all_gather x1 -> x0, blocking collectives: 8.13 us -> none  [on_device(): lax.all_gather(w_output, 'dp', axis=1, tiled=True)]
  transfers between devices with their start and end apart: 4 -> 0, of which waited for: 3 -> 0; matrix products, arithmetic and copies ran while one was open for 46% -> 0% of each run, Pallas kernels for 0% -> 0%
where the time goes in v5:
time: 156 us
  Pallas kernels  152 us (97%)
  local copies, waits for them, and re-layouts  2.52 us (2%)
  other arithmetic  1.83 us (1%)
    pallas_call x1, Pallas kernels, on_device(): pl.pallas_call(functools.partial(layer_kernel, heads, width, count, group...  152 us

profile of v5, /device:TPU:29, one launch (start us, length us, event | category | flops | bytes accessed | tf_op | source)
XLA Modules:
  0.0 156.2 jit_solution(12618242088514425663)
XLA Ops:
  0.0 1.8 %pad_maximum_fusion.stacked_ref = bf16[512,384]{1,0:T(8,128)(2,1)} fusion(bf16[512,128]{1,0:T(8,128)(2,1)} %param.10, bf16[512,128]{1,0:T(8,128)(2,1)} %param.9, bf16[512,128]{1,0:T(8,128)(2,1)} %param.8), kind=kLoop, calls=%fused_computation | loop fusion | flops 1179648 | bytes 786432 | tf_op jit(solution)/shard_map/concatenate | solution.py:256
  1.8 151.8 %shard_map.73 = bf16[320,2048]{1,0:T(8,128)(2,1)} custom-call(bf16[320,2048]{1,0:T(8,128)(2,1)} %bitcast.4, bf16[512,384]{1,0:T(8,128)(2,1)} %pad_maximum_fusion.stacked_ref, bf16[128,512]{1,0:T(8,128)(2,1)} %slab_ref.1, f32[2,64]{1,0:T(2,128)} %gain_ref.1, f32[2,2560]{1,0:T(2,128)} %bitcast.5), custom_call_target="tpu_custom_call" | custom-call | tf_op jit(solution)/shard_map/pallas_call | solution.py:260
  153.6 2.5 %copy.9 = bf16[1,320,2048]{2,1,0:T(8,128)(2,1)} copy(bf16[1,320,2048]{2,1,0:T(8,128)(2,1)} %bitcast.3) | data formatting | bytes 2621440

commit v6 on v5

--- a/solution.py
+++ b/solution.py
@@ -82,7 +82,9 @@
         ).astype(jnp.bfloat16)
 
     for step in range(count):
-        arrived = []
+        if step == min(2, count - 1):
+            for copy in weights:
+                copy.wait_recv()
         for piece in range(PIECES):
             for side, way in enumerate(ways):
                 offset = (side * PIECES + piece) * part
@@ -97,6 +99,10 @@
                     source, whole_ref.at[place], send_sem.at[step, piece, side],
                     recv_sem.at[step, piece, side], {"sp": targets[side]},
                 )
+            if 2 <= step < count - 1:
+                for place in backlog[:2]:
+                    project(place)
+                backlog = backlog[2:]
         for side, way in enumerate(ways):
             if step:
                 copies[step - 1, "slab", side].wait_recv()
@@ -129,13 +135,9 @@
             slabs_ref[group, pl.ds(pl.multiple_of(me * tall_slab, tall_slab), tall_slab), :] = (
                 slab_ref[...]
             )
-        if step == min(3, count - 1):
-            for copy in weights:
-                copy.wait_recv()
-        if step >= min(3, count - 1):
+        if step == count - 1:
             for place in backlog:
                 project(place)
-            backlog = []
 
 
     def remote(source, owner):

time: 156 us -> 157 us (level)
  no operation moved by 1% of the time
where the time goes in v6:
time: 157 us
  Pallas kernels  152 us (97%)
  local copies, waits for them, and re-layouts  2.52 us (2%)
  other arithmetic  1.83 us (1%)
    pallas_call x1, Pallas kernels, on_device(): pl.pallas_call(functools.partial(layer_kernel, heads, width, count, group...  152 us

profile of v6, /device:TPU:29, one launch (start us, length us, event | category | flops | bytes accessed | tf_op | source)
XLA Modules:
  0.0 156.9 jit_solution(12345794806590000207)
XLA Ops:
  0.0 1.8 %pad_maximum_fusion.stacked_ref = bf16[512,384]{1,0:T(8,128)(2,1)} fusion(bf16[512,128]{1,0:T(8,128)(2,1)} %param.10, bf16[512,128]{1,0:T(8,128)(2,1)} %param.9, bf16[512,128]{1,0:T(8,128)(2,1)} %param.8), kind=kLoop, calls=%fused_computation | loop fusion | flops 1179648 | bytes 786432 | tf_op jit(solution)/shard_map/concatenate | solution.py:258
  1.8 152.5 %shard_map.73 = bf16[320,2048]{1,0:T(8,128)(2,1)} custom-call(bf16[320,2048]{1,0:T(8,128)(2,1)} %bitcast.4, bf16[512,384]{1,0:T(8,128)(2,1)} %pad_maximum_fusion.stacked_ref, bf16[128,512]{1,0:T(8,128)(2,1)} %slab_ref.1, f32[2,64]{1,0:T(2,128)} %gain_ref.1, f32[2,2560]{1,0:T(2,128)} %bitcast.5), custom_call_target="tpu_custom_call" | custom-call | tf_op jit(solution)/shard_map/pallas_call | solution.py:262
  154.3 2.5 %copy.9 = bf16[1,320,2048]{2,1,0:T(8,128)(2,1)} copy(bf16[1,320,2048]{2,1,0:T(8,128)(2,1)} %bitcast.3) | data formatting | bytes 2621440
